TPU v7x, 512 devices: a whole 4x4x16 slice. The times are simulated.
512 devices in a mesh: ep: 32 (over z, core), tp: 16 (over y, x).
Axes of the slice: x: 4, y: 4, z: 16, core: 2. Of those that a mesh axis runs over, the one named last changes fastest.
Arguments:
- query_rows: bfloat16 [16384, 2048], P('ep', 'tp'), may hold values from -6 to 6
- key_rows: bfloat16 [16384, 2048], P('ep', 'tp'), may hold values from -6 to 6
- value_rows: bfloat16 [16384, 4096], P('ep', 'tp'), may hold values from -6 to 6
- in_gate: float32 [16, 16384], P('tp', 'ep'), may hold values from -120 to 120
- forget_gate: float32 [16, 16384], P('tp', 'ep'), may hold values from -2 to 20
- out_gate: bfloat16 [16384, 4096], P('ep', 'tp'), may hold values from -6 to 6
- head_gain: float32 [4096], P('tp'), may hold values from 0.1 to 1.9
- mix_weight: bfloat16 [4096, 4096], P(None, 'tp'), may hold values from -0.09375 to 0.09375
- expert_input: bfloat16 [8192, 4096], P('ep', 'tp'), may hold values from -30 to 30
- routes: int32 [8192, 2], P('ep'), may hold values from 0 to 31, all different within a row; in each aligned block of 256 rows (0 to 255, 256 to 511, ...) at most 32 rows name the same one
- route_weight: float32 [8192, 2], P('ep'), may hold values from 0.25 to 1.25
- gate_weight: bfloat16 [32, 1024, 4096], P('ep', 'tp'), may hold values from -0.09375 to 0.09375
- up_weight: bfloat16 [32, 1024, 4096], P('ep', 'tp'), may hold values from -0.09375 to 0.09375
- down_weight: bfloat16 [32, 1024, 4096], P('ep', None, 'tp'), may hold values from -0.1875 to 0.1875
Outputs:
- mixer_out: bfloat16 [16384, 4096], P('ep', 'tp')
- expert_out: bfloat16 [8192, 4096], P('ep', 'tp')
Inputs may be any that keep to these rules, and one draw needn't show every extreme that they name: `routes`: each row names 2 different experts. In the rows of one device no expert is named by more than 32 rows, and in the rows of some device an expert is named by exactly 32 rows.
All inputs are finite; a program needn't handle non-finite values.
Results may differ from a plain program's by a relative error of at most 0.0057.
Values may be sent and summed in bfloat16 or wider, within the bound.
No kernel may reach another device: no remote copies, remote signals or barrier semaphores. Data moves between devices by JAX's collectives and lax.ppermute only.
A program may use at most 128 MiB of HBM per device.

v0:
```python
import jax
import jax.numpy as jnp
from jax import lax
from jax.sharding import Mesh
from jax.sharding import PartitionSpec as P

D = 4096
BLOCK = 64
EP = ("ep_0", "ep_1")
EPSILON = 1e-06
LOG_FLOOR = -1e30
HIGHEST_PRECISION = lax.Precision.HIGHEST


def nothing_yet(x, identity):
    return jax.tree.map(
        lambda part, zero: jnp.zeros_like(part) + jnp.asarray(zero, part.dtype), x, identity
    )


def collected_together(x, axis):
    leaves = jax.tree.leaves(x)
    turns = sorted(range(len(leaves)), key=lambda k: -leaves[k].size)
    width = (1, *leaves[turns[0]].shape)[-1]
    lines = [
        jnp.pad(leaves[k].reshape(-1), (0, -leaves[k].size % width)).reshape(-1, width)
        for k in turns
    ]
    both, at, found = (lax.all_gather(jnp.concatenate(lines), axis), 0, {})
    for k, line in zip(turns, lines):
        share = both[:, at : at + len(line)].reshape(len(both), -1)
        found[k] = share[:, : leaves[k].size].reshape(-1, *leaves[k].shape)
        at += len(line)
    numbers = iter(range(len(leaves)))
    return jax.tree.map(lambda _: found[next(numbers)], x)


def prefix_by_axis(x, axes, combine, identity):
    before = start = nothing_yet(x, identity)
    subtotal = x
    for axis in reversed(axes):
        length, index = (lax.axis_size(axis), lax.axis_index(axis))
        pieces = collected_together(subtotal, axis)
        inside, subtotal = (start, start)
        for k in range(length):
            passed = k < index
            subtotal = combine(subtotal, jax.tree.map(lambda part: part[k], pieces))
            inside = jax.tree.map(lambda new, old: jnp.where(passed, new, old), subtotal, inside)
        before = combine(inside, before)
    return before


def joined_along(tiles, dim):
    dims = list(tiles.shape[1:])
    dims[dim] *= tiles.shape[0]
    return jnp.moveaxis(tiles, 0, dim).reshape(dims)


def copy_for_each(x, axis):
    copies = jnp.broadcast_to(x, (lax.axis_size(axis), *x.shape))
    return lax.all_to_all(copies, axis, split_axis=0, concat_axis=0, tiled=True)


def gather_directly(x, axis, dim):
    return joined_along(copy_for_each(x, axis), dim)


def combine(first_part, second_part):
    decay_first, max_first, memory_first, normal_first = first_part
    decay_second, max_second, memory_second, normal_second = second_part
    running_max = jnp.maximum(decay_second + max_first, max_second)
    keep_first = jnp.exp(decay_second + max_first - running_max)
    keep_second = jnp.exp(max_second - running_max)
    memory = (
        keep_first[..., None, None] * memory_first + keep_second[..., None, None] * memory_second
    )
    normalizer = keep_first[..., None] * normal_first + keep_second[..., None] * normal_second
    return (decay_first + decay_second, running_max, memory, normalizer)


def identity_state(head_count, key_width, value_width):
    return (
        jnp.zeros((head_count,), jnp.float32),
        jnp.full((head_count,), LOG_FLOOR, jnp.float32),
        jnp.zeros((head_count, key_width, value_width), jnp.float32),
        jnp.zeros((head_count, key_width), jnp.float32),
    )


def halfprod(form, left, right):
    return jnp.einsum(form, left, right, preferred_element_type=jnp.float32)


def prepare(query_heads, key_heads, value_heads, in_gate, forget_gate):
    head_count, length, key_width = query_heads.shape
    block_count = length // BLOCK
    query_blocks = query_heads.reshape(head_count, block_count, BLOCK, key_width)
    key_blocks = key_heads.reshape(head_count, block_count, BLOCK, key_width)
    value_blocks = value_heads.reshape(head_count, block_count, BLOCK, value_heads.shape[-1])
    log_input = in_gate.reshape(head_count, block_count, BLOCK)
    cumulative = jnp.cumsum(
        jax.nn.log_sigmoid(forget_gate).reshape(head_count, block_count, BLOCK), axis=-1
    )
    block_decay = cumulative[..., -1]
    weight_log = block_decay[..., None] - cumulative + log_input
    block_max = jnp.max(weight_log, axis=-1)
    weighted = (
        key_blocks.astype(jnp.float32) * jnp.exp(weight_log - block_max[..., None])[..., None]
    )
    normalizer = jnp.sum(weighted, axis=2)
    memory = halfprod("hcsk,hcsv->hckv", weighted.astype(jnp.bfloat16), value_blocks)
    return (
        (query_blocks, key_blocks, value_blocks, log_input, cumulative),
        (block_decay, block_max, memory, normalizer),
    )


def prefix(summary, initial):
    leading = jax.tree.map(lambda tensor: jnp.moveaxis(tensor, 1, 0), summary)

    def advance(running, current):
        return (combine(running, current), running)

    final_state, before = lax.scan(advance, initial, leading)
    return (final_state, jax.tree.map(lambda tensor: jnp.moveaxis(tensor, 0, 1), before))


def block_outputs(blocked, before):
    query_blocks, key_blocks, value_blocks, log_input, cumulative = blocked
    prior_max, prior_memory, prior_normal = (before[1], before[2], before[3])
    block_len = cumulative.shape[-1]
    scale = query_blocks.shape[-1] ** (-0.5)
    causal = jnp.tril(jnp.ones((block_len, block_len), dtype=bool))
    log_decay = jnp.where(
        causal,
        cumulative[..., :, None] - cumulative[..., None, :] + log_input[..., None, :],
        -jnp.inf,
    )
    log_inter = cumulative + prior_max[..., None]
    top_value = jnp.maximum(log_inter, jnp.max(log_decay, axis=-1))
    scores = (
        halfprod("hctk,hcsk->hcts", query_blocks, key_blocks)
        * scale
        * jnp.exp(log_decay - top_value[..., None])
    )
    carried = jnp.exp(log_inter - top_value) * scale
    query_wide = query_blocks.astype(jnp.float32)
    numerator = carried[..., None] * jnp.einsum(
        "hctk,hckv->hctv", query_wide, prior_memory, precision=HIGHEST_PRECISION
    ) + halfprod("hcts,hcsv->hctv", scores.astype(jnp.bfloat16), value_blocks)
    denominator = carried * jnp.einsum(
        "hctk,hck->hct", query_wide, prior_normal, precision=HIGHEST_PRECISION
    ) + jnp.sum(scores, axis=-1)
    return numerator / jnp.maximum(jnp.abs(denominator), jnp.exp(-top_value))[..., None]


def finish(head_values, out_gate, head_gain):
    head_count, block_count, block_len, value_width = head_values.shape
    per_head = jnp.transpose(head_values, (1, 2, 0, 3)).reshape(
        block_count * block_len, head_count, value_width
    )
    per_head = per_head * lax.rsqrt(jnp.mean(per_head * per_head, axis=-1, keepdims=True) + EPSILON)
    per_head = per_head.reshape(block_count * block_len, head_count * value_width) * head_gain
    per_head = per_head * jax.nn.sigmoid(out_gate.astype(jnp.float32))
    return per_head.astype(jnp.bfloat16)


def cell_heads(query_rows, key_rows, value_rows, in_gate, forget_gate, out_gate, head_gain):
    length = query_rows.shape[0]
    head_count = in_gate.shape[0]
    key_width = query_rows.shape[1] // head_count
    value_width = value_rows.shape[1] // head_count
    query_heads = query_rows.reshape(length, head_count, key_width).transpose(1, 0, 2)
    key_heads = key_rows.reshape(length, head_count, key_width).transpose(1, 0, 2)
    value_heads = value_rows.reshape(length, head_count, value_width).transpose(1, 0, 2)
    blocked, summary = prepare(query_heads, key_heads, value_heads, in_gate, forget_gate)
    initial = identity_state(head_count, key_width, value_width)
    final_state, before = prefix(summary, initial)
    incoming = prefix_by_axis(final_state, EP, combine, initial)
    expanded = jax.tree.map(lambda tensor: tensor[:, None], incoming)
    before = combine(expanded, before)
    return finish(block_outputs(blocked, before), out_gate, head_gain)


def body(
    query_rows,
    key_rows,
    value_rows,
    in_gate,
    forget_gate,
    out_gate,
    head_gain,
    mix_weight,
    expert_input,
    routes,
    route_weight,
    gate_weight,
    up_weight,
    down_weight,
):
    mixed_heads = cell_heads(
        query_rows, key_rows, value_rows, in_gate, forget_gate, out_gate, head_gain
    )
    gate_local = gate_weight[0]
    up_local = up_weight[0]
    down_local = down_weight[0]
    group_size = lax.axis_size(EP)
    token_count, fanout = routes.shape
    capacity = 2 * token_count * fanout // group_size
    slot_count = group_size * capacity
    chosen = routes.reshape(-1)
    one_hot = (chosen[:, None] == jnp.arange(group_size, dtype=jnp.int32)[None, :]).astype(
        jnp.int32
    )
    position = jnp.sum((jnp.cumsum(one_hot, axis=0) - one_hot) * one_hot, axis=1)
    target = chosen * capacity + position
    matches = (jnp.arange(slot_count, dtype=jnp.int32)[:, None] == target[None, :]).astype(
        jnp.int32
    )
    occupied = jnp.sum(matches, axis=1) > 0
    source_row = jnp.sum(
        matches * (jnp.arange(token_count * fanout, dtype=jnp.int32) // fanout)[None, :], axis=1
    )
    arrived = lax.all_to_all(
        jnp.where(
            occupied[:, None],
            jnp.take(expert_input, source_row, axis=0),
            jnp.zeros((), expert_input.dtype),
        ),
        EP,
        split_axis=0,
        concat_axis=0,
        tiled=True,
    )
    head_piece = lax.all_gather(mixed_heads, "tp", axis=1, tiled=True)
    token_piece = lax.all_gather(arrived, "tp", axis=1, tiled=True)
    mix_acc = jnp.dot(head_piece, mix_weight, preferred_element_type=jnp.float32)
    gate_acc = jnp.einsum("sd,fd->sf", token_piece, gate_local, preferred_element_type=jnp.float32)
    up_acc = jnp.einsum("sd,fd->sf", token_piece, up_local, preferred_element_type=jnp.float32)
    squares = jnp.sum(jnp.square(token_piece.astype(jnp.float32)), axis=1)
    mix_acc, gate_acc, up_acc, squares = (mix_acc, gate_acc, up_acc, squares)
    mixer_out = mix_acc.astype(jnp.bfloat16)
    inverse_rms = lax.rsqrt(squares / D + EPSILON)[:, None]
    hidden = (jax.nn.silu(gate_acc * inverse_rms) * (up_acc * inverse_rms)).astype(jnp.bfloat16)
    expert_rows = jnp.dot(
        gather_directly(hidden, "tp", 1), down_local, preferred_element_type=jnp.float32
    )
    returned_rows = lax.all_to_all(
        expert_rows.astype(jnp.bfloat16), EP, split_axis=0, concat_axis=0, tiled=True
    )
    picked_rows = (
        jnp.take(returned_rows, target, axis=0).reshape(token_count, fanout, -1).astype(jnp.float32)
    )
    expert_out = jnp.sum(picked_rows * route_weight[:, :, None], axis=1).astype(jnp.bfloat16)
    return (mixer_out, expert_out)


def solution(mesh):
    split = Mesh(mesh.devices.reshape(16, 2, mesh.shape["tp"]), ("ep_0", "ep_1", "tp"))
    in_specs = (
        P(EP, "tp"),
        P(EP, "tp"),
        P(EP, "tp"),
        P("tp", EP),
        P("tp", EP),
        P(EP, "tp"),
        P("tp"),
        P(None, "tp"),
        P(EP, "tp"),
        P(EP, None),
        P(EP, None),
        P(EP, "tp", None),
        P(EP, "tp", None),
        P(EP, None, "tp"),
    )
    out_specs = (P(EP, "tp"), P(EP, "tp"))
    return jax.shard_map(body, mesh=split, in_specs=in_specs, out_specs=out_specs, check_vma=False)
```

profile of v0, /device:TPU:1, one launch (start us, length us, event | category | flops | bytes accessed | tf_op | source)
XLA Modules:
  0.0 352.5 jit_solution(5622983685871281707)
XLA Ops:
  9.1 1.3 reduce.22
  11.6 1.1 fusion.21
  12.6 1.5 convolution_bitcast_fusion
  14.2 36.5 %while.25 = (s32[]{:T(128)}, f32[1]{0:T(128)}, f32[1]{0:T(128)}, f32[1,128,256]{2,1,0:T(8,128)S(1)}, f32[1,128]{1,0:T(1,128)S(1)}, /*index=5*/f32[8,1]{0,1:T(1,1...) while((s32[]{:T(128)}, f32[1]{0:T(128)}, f32[1]{0:T(128)}, ...), condition=%wide.region_4.5_spmd.clone, body=%wide.region_3.4_spmd.clone.sunk | while | flops 164488 | bytes 659258 | solution.py:124
  51.2 8.5 %all-gather.2 = f32[2,131,256]{2,1,0:T(8,128)S(1)} all-gather(f32[1,131,256]{2,1,0:T(8,128)S(1)} %maximum_bitcast_fusion), channel_id=2, replica_groups=mesh['ep_0'=16,'ep_1'=2,'tp'=16] {'ep_1'}, dimensions={0}, use_global_device_ids=true | all-gather | bytes 402432 | tf_op jit(solution)/shard_map/all_gather | solution.py:29
  68.1 1.2 reduce-window.6
  70.5 3.9 %gather_fusion = bf16[1024,256]{1,0:T(8,128)(2,1)S(1)} fusion(bf16[256,256]{1,0:T(8,128)(2,1)S(1)} %copy-done.1, s32[1024]{0:T(1024)S(1)} %broadcast_clamp_fusion), kind=kCustom, calls=%fused_computation | custom fusion | bytes 1052672 | tf_op jit(solution)/shard_map/jit(_take)/gather | solution.py:227
  74.9 48.4 %all_to_all.26 = bf16[32,32,256]{2,1,0:T(8,128)(2,1)} all-to-all(bf16[32,32,256]{2,1,0:T(8,128)(2,1)S(1)} %select_select_fusion), channel_id=1, replica_groups=mesh['ep_0'=16,'ep_1'=2,'tp'=16] {'ep_0','ep_1'}, dimensions={0} | all-to-all | bytes 1048576 | tf_op jit(solution)/shard_map/all_to_all | solution.py:224
  124.7 22.1 %all-gather.12.cloned.1.call-done = f32[16,131,256]{2,1,0:T(8,128)} async-done(((f32[1,131,256]{2,1,0:T(8,128)}), f32[16,131,256]{2,1,0:T(8,128)}) %all-gather.12.cloned.1.call-update) | async-done | bytes 2146320 | tf_op jit(solution)/shard_map/all_gather | solution.py:29
  146.8 1.1 fusion.82
  181.0 2.0 fusion.26
  184.2 0.9 fusion.17
  185.1 59.3 %all-gather.10.cloned.1.call-done = bf16[1024,4096]{1,0:T(8,128)(2,1)} async-done(((bf16[1024,256]{1,0:T(8,128)(2,1)}), bf16[1024,4096]{1,0:T(8,128)(2,1)}) %all-gather.10.cloned.1.call-update) | async-done | bytes 8388624 | tf_op jit(solution)/shard_map/all_gather | solution.py:236
  244.4 5.2 %multiply_reduce_fusion = f32[1024]{0:T(1024)S(1)} fusion(bf16[1024,4096]{1,0:T(8,128)(2,1)} %all-gather.10.cloned.1.call-done), kind=kLoop, calls=%fused_computation.12 | loop fusion | flops 12581888 | bytes 8392704 | tf_op jit(solution)/shard_map/reduce_sum | solution.py:240
  250.1 2.7 convolution_multiply_fusion.3
  252.8 2.7 fusion.8
  255.8 35.5 %all_to_all.27 = bf16[16,1024,64]{1,2,0:T(8,128)(2,1)S(1)} all-to-all(bf16[16,1024,64]{1,2,0:T(8,128)(2,1)S(1)} %broadcast_in_dim.75), channel_id=1, replica_groups=mesh['ep_0'=16,'ep_1'=2,'tp'=16] {'tp'}, dimensions={0} | all-to-all | bytes 4194304 | tf_op jit(solution)/shard_map/all_to_all | solution.py:61
  291.3 1.6 convolution_convert_fusion
  292.9 15.3 %all-to-all-start.2 = ((bf16[32,32,256]{2,1,0:T(8,128)(2,1)}), bf16[32,32,256]{2,1,0:T(8,128)(2,1)S(1)}, u32[]{:S(2)}, u32[]{:S(2)}) async-start(bf16[32,32,256]{2,1,0:T(8,128)(2,1)} %bitcast.139), calls=%async_computation.2 | async-start | bytes 1048576 | tf_op jit(solution)/shard_map/all_to_all | solution.py:248
  309.1 22.7 %all-gather.8.cloned.1.call-done = bf16[512,4096]{1,0:T(8,128)(2,1)} async-done(((bf16[512,256]{1,0:T(8,128)(2,1)}), bf16[512,4096]{1,0:T(8,128)(2,1)}) %all-gather.8.cloned.1.call-update) | async-done | bytes 4194320 | tf_op jit(solution)/shard_map/all_gather | solution.py:235
  331.8 4.1 %convolution_convert_fusion.1 = bf16[512,256]{1,0:T(8,128)(2,1)} fusion(bf16[512,4096]{1,0:T(8,128)(2,1)} %all-gather.8.cloned.1.call-done, bf16[4096,256]{1,0:T(8,128)(2,1)S(1)} %copy-done), kind=kOutput, calls=%fused_computation.22 | convolution fusion | flops 1073872896 | bytes 6553600 | tf_op jit(solution)/shard_map/dot_general | solution.py:237
  335.9 5.8 %all-to-all-done.2 = bf16[32,32,256]{2,1,0:T(8,128)(2,1)S(1)} async-done(((bf16[32,32,256]{2,1,0:T(8,128)(2,1)}), bf16[32,32,256]{2,1,0:T(8,128)(2,1)S(1)}, u32[]{:S(2)}, u32[]{:S(2)}) %all-to-all-start.2) | async-done | bytes 524320 | tf_op jit(solution)/shard_map/all_to_all | solution.py:248
  341.7 1.9 gather_fusion.1
  343.8 2.2 multiply_reduce_fusion.1
  (190 shorter events, 30.6 us)
Async XLA Ops:
  7.2 324.6 %copy-start = (bf16[4096,256]{1,0:T(8,128)(2,1)S(1)}, bf16[4096,256]{1,0:T(8,128)(2,1)}, u32[]{:S(2)}) copy-start(bf16[4096,256]{1,0:T(8,128)(2,1)} %param.23) | copy-start | bytes 6291460
  7.2 139.6 %all-gather.12.cloned.1.call-start = ((), (), s32[]{:S(2)}) async-start(), calls=%async_computation.5 | async-start | bytes 2367488 | tf_op jit(solution)/shard_map/all_gather | solution.py:29
  8.4 5.7 %copy-start.7 = (f32[1,8,64]{2,1,0:T(8,128)}, f32[1,8,64]{2,1,0:T(8,128)S(1)}, u32[]{:S(2)}) copy-start(f32[1,8,64]{2,1,0:T(8,128)S(1)} %reduce_window_sum.28) | copy-start | bytes 6148
  11.3 2.8 copy-start.9
  14.1 56.4 %copy-start.1 = (bf16[256,256]{1,0:T(8,128)(2,1)S(1)}, bf16[256,256]{1,0:T(8,128)(2,1)}, u32[]{:S(2)}) copy-start(bf16[256,256]{1,0:T(8,128)(2,1)} %param.24) | copy-start | bytes 393220
  67.0 177.4 %all-gather.10.cloned.1.call-start = ((), (), s32[]{:S(2)}) async-start(), calls=%async_computation.4 | async-start | bytes 8912896 | tf_op jit(solution)/shard_map/all_gather | solution.py:236
  74.5 49.9 %copy-start.8 = (f32[1,8,64]{2,1,0:T(8,128)S(1)}, f32[1,8,64]{2,1,0:T(8,128)}, u32[]{:S(2)}) copy-start(f32[1,8,64]{2,1,0:T(8,128)} %copy-done.7) | copy-start | bytes 6148
  74.5 49.9 %copy-start.10 = (f32[8,64]{1,0:T(8,128)S(1)}, f32[8,64]{1,0:T(8,128)}, u32[]{:S(2)}) copy-start(f32[8,64]{1,0:T(8,128)} %copy-done.9) | copy-start | bytes 6148
  74.5 105.5 %copy-start.16 = (f32[8,1]{0,1:T(1,128)S(1)}, f32[8,1]{0,1:T(1,128)}, u32[]{:S(2)}) copy-start(f32[8,1]{0,1:T(1,128)} %copy-done.15) | copy-start | bytes 100
  74.5 105.5 %copy-start.18 = (f32[8,1]{0,1:T(1,128)S(1)}, f32[8,1]{0,1:T(1,128)}, u32[]{:S(2)}) copy-start(f32[8,1]{0,1:T(1,128)} %copy-done.17) | copy-start | bytes 100
  74.5 105.7 %copy-start.12 = (f32[8,1,128]{2,1,0:T(1,128)S(1)}, f32[8,1,128]{2,1,0:T(1,128)}, u32[]{:S(2)}) copy-start(f32[8,1,128]{2,1,0:T(1,128)} %get-tuple-element.83) | copy-start | bytes 12292
  74.5 105.8 %copy-start.22 = (bf16[512,128]{1,0:T(8,128)(2,1)S(1)}, bf16[512,128]{1,0:T(8,128)(2,1)}, u32[]{:S(2)}) copy-start(bf16[512,128]{1,0:T(8,128)(2,1)} %param.16) | copy-start | bytes 393220
  74.5 106.1 %copy-start.5 = (bf16[512,128]{1,0:T(8,128)(2,1)S(1)}, bf16[512,128]{1,0:T(8,128)(2,1)}, u32[]{:S(2)}) copy-start(bf16[512,128]{1,0:T(8,128)(2,1)} %param.17) | copy-start | bytes 393220
  123.3 59.7 %copy-start.3 = (bf16[512,256]{1,0:T(8,128)(2,1)S(1)}, bf16[512,256]{1,0:T(8,128)(2,1)}, u32[]{:S(2)}) copy-start(bf16[512,256]{1,0:T(8,128)(2,1)} %param.18) | copy-start | bytes 786436
  123.3 208.4 %all-gather.8.cloned.1.call-start = ((), (), s32[]{:S(2)}) async-start(), calls=%async_computation.3 | async-start | bytes 4456448 | tf_op jit(solution)/shard_map/all_gather | solution.py:235
  180.3 3.0 copy-start.19
  180.3 3.0 copy-start.23
  184.2 65.4 %copy-start.4 = (bf16[1,64,4096]{2,1,0:T(8,128)(2,1)S(1)}, bf16[1,64,4096]{2,1,0:T(8,128)(2,1)}, u32[]{:S(2)}) copy-start(bf16[1,64,4096]{2,1,0:T(8,128)(2,1)} %param.27) | copy-start | bytes 1572868
  244.4 5.8 %copy-start.2 = (bf16[1024,4096]{1,0:T(8,128)(2,1)S(1)}, bf16[1024,4096]{1,0:T(8,128)(2,1)}, u32[]{:S(2)}) copy-start(bf16[1024,4096]{1,0:T(8,128)(2,1)} %all-gather.10.cloned.1.call-done) | copy-start | bytes 25165828
  250.1 2.7 copy-start.20
  255.8 35.5 %copy-start.21 = (bf16[1,1024,256]{2,1,0:T(8,128)(2,1)S(1)}, bf16[1,1024,256]{2,1,0:T(8,128)(2,1)}, u32[]{:S(2)}) copy-start(bf16[1,1024,256]{2,1,0:T(8,128)(2,1)} %param.29) | copy-start | bytes 1572868
  291.3 17.0 %copy-start.11 = (s32[256,2]{0,1:T(2,128)S(1)}, s32[256,2]{0,1:T(2,128)}, u32[]{:S(2)}) copy-start(s32[256,2]{0,1:T(2,128)} %param.25) | copy-start | bytes 6148
  291.3 17.6 %copy-start.13 = (f32[256,2]{0,1:T(2,128)S(1)}, f32[256,2]{0,1:T(2,128)}, u32[]{:S(2)}) copy-start(f32[256,2]{0,1:T(2,128)} %param.26) | copy-start | bytes 6148
  292.9 48.8 %all-to-all-start.2 = ((bf16[32,32,256]{2,1,0:T(8,128)(2,1)}), bf16[32,32,256]{2,1,0:T(8,128)(2,1)S(1)}, u32[]{:S(2)}, u32[]{:S(2)}) async-start(bf16[32,32,256]{2,1,0:T(8,128)(2,1)} %bitcast.139), calls=%async_computation.2 | async-start | bytes 1048576 | tf_op jit(solution)/shard_map/all_to_all | solution.py:248
  (4 other events, 3.5 us)
Sparse Core Ops, SparseCore 0:
  67.1 79.6 all-gather.11
  149.7 94.5 all-gather.9
  247.9 83.7 all-gather.7
where the time goes:
time: 354 us; the launch traced here: 352 us
  waiting for transfers between devices  110 us (31%)
  blocking collectives  92.4 us (26%)
  between operations  51.3 us (14%)
  other arithmetic  28 us (8%)
  local copies, waits for them, and re-layouts  21.5 us (6%)
  loops' own time  19.7 us (6%)
  starting transfers between devices  15.6 us (4%)
  matrix products  14.2 us (4%)
    all_gather x1, waiting for transfers between devices, body(): token_piece = lax.all_gather(arrived, 'tp', axis=1, tiled=True)  59.3 us
    all_to_all x1, blocking collectives, body(): lax.all_to_all(jnp.where(occupied[:, None], jnp.take(expert_input, source...  48.4 us
    all_to_all x1, blocking collectives, copy_for_each(): return lax.all_to_all(copies, axis, split_axis=0, concat_axis=0, tiled=True)  35.5 us
    all_gather x1, waiting for transfers between devices, body(): head_piece = lax.all_gather(mixed_heads, 'tp', axis=1, tiled=True)  22.7 us
    all_gather x1, waiting for transfers between devices, collected_together(): both, at, found = (lax.all_gather(jnp.concatenate(lines), axis), 0, {})  22.1 us
    another operation x1, loops' own time, prefix(): final_state, before = lax.scan(advance, initial, leading)  19.7 us
    all_to_all x1, starting transfers between devices, body(): lax.all_to_all(expert_rows.astype(jnp.bfloat16), EP, split_axis=0, concat...  15.3 us
    dynamic_update_slice x16, other arithmetic, prefix(): final_state, before = lax.scan(advance, initial, leading)  9.85 us
  transfers between devices with their start and end apart: 4, of which 4 were waited for; matrix products, arithmetic and copies ran while one was open for 9% of the time, Pallas kernels for 0%

commit v1 on v0

--- a/solution.py
+++ b/solution.py
@@ -10,6 +10,11 @@
 EPSILON = 1e-06
 LOG_FLOOR = -1e30
 HIGHEST_PRECISION = lax.Precision.HIGHEST
+
+
+def gather_from_all(x, axis, dim):
+    copies = jnp.concatenate([x] * lax.axis_size(axis), axis=dim)
+    return lax.all_to_all(copies, axis, dim, dim, tiled=True)
 
 
 def nothing_yet(x, identity):
@@ -233,7 +238,7 @@
         tiled=True,
     )
     head_piece = lax.all_gather(mixed_heads, "tp", axis=1, tiled=True)
-    token_piece = lax.all_gather(arrived, "tp", axis=1, tiled=True)
+    token_piece = gather_from_all(arrived, "tp", 1)
     mix_acc = jnp.dot(head_piece, mix_weight, preferred_element_type=jnp.float32)
     gate_acc = jnp.einsum("sd,fd->sf", token_piece, gate_local, preferred_element_type=jnp.float32)
     up_acc = jnp.einsum("sd,fd->sf", token_piece, up_local, preferred_element_type=jnp.float32)

time: 354 us -> 374 us (1.056)
  blocking collectives: 92.4 us -> 39.6 us
  local copies, waits for them, and re-layouts: 21.5 us -> 62.2 us
  starting transfers between devices: 15.6 us -> 37.6 us
  waiting for transfers between devices: 110 us -> 116 us
  other arithmetic: 28 us -> 31.9 us
    all_gather x1 -> x0, waiting for transfers between devices: 59.3 us -> none  [body(): token_piece = lax.all_gather(arrived, 'tp', axis=1, tiled=True)]
    all_to_all x1 -> x0, blocking collectives: 48.4 us -> none  [body(): lax.all_to_all(jnp.where(occupied[:, None], jnp.take(expert_input, source...]
    all_to_all x0 -> x2, waiting for transfers between devices: none -> 35.2 us  [the longest x1 35.2 us: gather_from_all(): return lax.all_to_all(copies, axis, dim, dim, tiled=True)]
    all_gather x1, waiting for transfers between devices: 22.1 us -> 52 us  [collected_together(): both, at, found = (lax.all_gather(jnp.concatenate(lines), axis), 0, {})]
    all_to_all x0 -> x2, starting transfers between devices: none -> 23.7 us  [the longest x1 16.8 us: body(): lax.all_to_all(jnp.where(occupied[:, None], jnp.take(expert_input, source...]
    all_gather x1, waiting for transfers between devices: 22.7 us -> 0.02 us  [body(): head_piece = lax.all_gather(mixed_heads, 'tp', axis=1, tiled=True)]
    all_to_all x1, waiting for transfers between devices: 5.79 us -> 28.4 us  [body(): lax.all_to_all(expert_rows.astype(jnp.bfloat16), EP, split_axis=0, concat...]
    dynamic_update_slice x16, local copies, waits for them, and re-layouts: 1.57 us -> 20.2 us  [prefix(): final_state, before = lax.scan(advance, initial, leading)]
  transfers between devices with their start and end apart: 4 -> 5, of which waited for: 4 -> 3; matrix products, arithmetic and copies ran while one was open for 9% -> 25% of each run, Pallas kernels for 0% -> 0%
where the time goes in v1:
time: 374 us; the launch traced here: 371 us
  waiting for transfers between devices  116 us (31%)
  local copies, waits for them, and re-layouts  62.2 us (17%)
  between operations  51.9 us (14%)
  blocking collectives  39.6 us (11%)
  starting transfers between devices  37.6 us (10%)
  other arithmetic  31.9 us (9%)
  loops' own time  19.9 us (5%)
  matrix products  11.9 us (3%)
    all_gather x1, waiting for transfers between devices, collected_together(): both, at, found = (lax.all_gather(jnp.concatenate(lines), axis), 0, {})  52 us
    all_to_all x1, blocking collectives, copy_for_each(): return lax.all_to_all(copies, axis, split_axis=0, concat_axis=0, tiled=True)  37.6 us
    all_to_all x1, waiting for transfers between devices, gather_from_all(): return lax.all_to_all(copies, axis, dim, dim, tiled=True)  35.2 us
    all_to_all x1, waiting for transfers between devices, body(): lax.all_to_all(expert_rows.astype(jnp.bfloat16), EP, split_axis=0, concat...  28.4 us
    dynamic_update_slice x16, local copies, waits for them, and re-layouts, prefix(): final_state, before = lax.scan(advance, initial, leading)  20.2 us
    another operation x1, loops' own time, prefix(): final_state, before = lax.scan(advance, initial, leading)  19.9 us
    all_to_all x1, starting transfers between devices, body(): lax.all_to_all(jnp.where(occupied[:, None], jnp.take(expert_input, source...  16.8 us
    all_to_all x1, starting transfers between devices, body(): lax.all_to_all(expert_rows.astype(jnp.bfloat16), EP, split_axis=0, concat...  13.6 us
  transfers between devices with their start and end apart: 5, of which 3 were waited for; matrix products, arithmetic and copies ran while one was open for 25% of the time, Pallas kernels for 0%

profile of v1, /device:TPU:1, one launch (start us, length us, event | category | flops | bytes accessed | tf_op | source)
XLA Modules:
  0.0 370.7 jit_solution(8734828979158458771)
XLA Ops:
  10.9 3.9 %gather_fusion = bf16[1024,256]{1,0:T(8,128)(2,1)S(1)} fusion(bf16[256,256]{1,0:T(8,128)(2,1)S(1)} %copy-done.2, s32[1024]{0:T(1024)S(1)} %broadcast_clamp_fusion), kind=kCustom, calls=%fused_computation | custom fusion | bytes 1052672 | tf_op jit(solution)/shard_map/jit(_take)/gather | solution.py:232
  16.0 16.8 %all-to-all-start = ((bf16[32,32,256]{2,1,0:T(8,128)(2,1)}), bf16[32,32,256]{2,1,0:T(8,128)(2,1)}, u32[]{:S(2)}, u32[]{:S(2)}) async-start(bf16[32,32,256]{2,1,0:T(8,128)(2,1)} %select_select_fusion), calls=%async_computation | async-start | bytes 1048576 | tf_op jit(solution)/shard_map/all_to_all | solution.py:229
  35.8 1.4 convolution_bitcast_fusion
  37.2 65.9 %while.25 = (s32[]{:T(128)}, f32[1]{0:T(128)}, f32[1]{0:T(128)}, f32[1,128,256]{2,1,0:T(8,128)S(1)}, f32[1,128]{1,0:T(1,128)S(1)}, /*index=5*/f32[8,1]{0,1:T(1,1...) while((s32[]{:T(128)}, f32[1]{0:T(128)}, f32[1]{0:T(128)}, ...), condition=%wide.region_4.5_spmd.clone, body=%wide.region_3.4_spmd.clone.sunk | while | flops 164488 | bytes 659258 | solution.py:129
  52.2 1.4 dynamic_update_slice.28
  85.2 1.4 dynamic_update_slice.28
  93.5 1.4 dynamic_update_slice.28
  103.1 2.0 all-gather.2
  112.3 5.1 %concatenate.15 = bf16[1024,16,256]{2,0,1:T(8,128)(2,1)} broadcast(bf16[1024,256]{1,0:T(8,128)(2,1)} %bitcast.133), dimensions={0,2} | broadcast | bytes 8912896 | tf_op jit(solution)/shard_map/concatenate | solution.py:16
  117.4 7.0 %all-to-all-start.1 = ((bf16[1024,16,256]{2,0,1:T(8,128)(2,1)}), bf16[1024,16,256]{2,0,1:T(8,128)(2,1)}, u32[]{:S(2)}, u32[]{:S(2)}) async-start(bf16[1024,16,256]{2,0,1:T(8,128)(2,1)} %concatenate.15), calls=%async_computation.1 | async-start | bytes 16777216 | tf_op jit(solution)/shard_map/all_to_all | solution.py:17
  125.8 52.0 %all-gather.9.cloned.1.call-done = f32[16,131,256]{2,1,0:T(8,128)} async-done(((f32[1,131,256]{2,1,0:T(8,128)}), f32[16,131,256]{2,1,0:T(8,128)}) %all-gather.9.cloned.1.call-update) | async-done | bytes 2146320 | tf_op jit(solution)/shard_map/all_gather | solution.py:34
  212.4 2.0 fusion.26
  216.6 35.2 %all-to-all-done.1 = bf16[1024,16,256]{2,0,1:T(8,128)(2,1)} async-done(((bf16[1024,16,256]{2,0,1:T(8,128)(2,1)}), bf16[1024,16,256]{2,0,1:T(8,128)(2,1)}, u32[]{:S(2)}, u32[]{:S(2)}) %all-to-all-start.1) | async-done | bytes 8388640 | tf_op jit(solution)/shard_map/all_to_all | solution.py:17
  251.7 12.3 %copy.70 = bf16[1024,16,256]{0,2,1:T(8,128)(2,1)} copy(bf16[1024,16,256]{2,0,1:T(8,128)(2,1)} %all-to-all-done.1) | data formatting | bytes 16777216 | tf_op jit(solution)/shard_map/all_to_all | solution.py:17
  264.1 5.2 %multiply_reduce_fusion = f32[1024]{0:T(1024)S(1)} fusion(bf16[1024,16,256]{2,0,1:T(8,128)(2,1)} %all-to-all-done.1), kind=kLoop, calls=%fused_computation.12 | loop fusion | flops 12581888 | bytes 8392704 | tf_op jit(solution)/shard_map/reduce_sum | solution.py:245
  269.8 1.6 convolution_multiply_fusion.3
  271.5 1.6 fusion.8
  273.4 37.6 %all_to_all.32 = bf16[16,1024,64]{1,2,0:T(8,128)(2,1)S(1)} all-to-all(bf16[16,1024,64]{1,2,0:T(8,128)(2,1)S(1)} %broadcast_in_dim.75), channel_id=1, replica_groups=mesh['ep_0'=16,'ep_1'=2,'tp'=16] {'tp'}, dimensions={0} | all-to-all | bytes 4194304 | tf_op jit(solution)/shard_map/all_to_all | solution.py:66
  310.9 1.6 convolution_convert_fusion
  312.5 13.6 %all-to-all-start.3 = ((bf16[32,32,256]{2,1,0:T(8,128)(2,1)}), bf16[32,32,256]{2,1,0:T(8,128)(2,1)S(1)}, u32[]{:S(2)}, u32[]{:S(2)}) async-start(bf16[32,32,256]{2,1,0:T(8,128)(2,1)} %bitcast.140), calls=%async_computation.3 | async-start | bytes 1048576 | tf_op jit(solution)/shard_map/all_to_all | solution.py:253
  327.1 4.1 %convolution_convert_fusion.1 = bf16[512,256]{1,0:T(8,128)(2,1)} fusion(bf16[512,4096]{1,0:T(8,128)(2,1)} %all-gather.7.cloned.1.call-done, bf16[4096,256]{1,0:T(8,128)(2,1)S(1)} %copy-done), kind=kOutput, calls=%fused_computation.22 | convolution fusion | flops 1073872896 | bytes 6553600 | tf_op jit(solution)/shard_map/dot_general | solution.py:242
  331.2 28.4 %all-to-all-done.3 = bf16[32,32,256]{2,1,0:T(8,128)(2,1)S(1)} async-done(((bf16[32,32,256]{2,1,0:T(8,128)(2,1)}), bf16[32,32,256]{2,1,0:T(8,128)(2,1)S(1)}, u32[]{:S(2)}, u32[]{:S(2)}) %all-to-all-start.3) | async-done | bytes 524320 | tf_op jit(solution)/shard_map/all_to_all | solution.py:253
  359.6 1.9 gather_fusion.1
  361.7 2.2 multiply_reduce_fusion.1
  (188 shorter events, 59.3 us)
Async XLA Ops:
  7.2 319.9 %copy-start = (bf16[4096,256]{1,0:T(8,128)(2,1)S(1)}, bf16[4096,256]{1,0:T(8,128)(2,1)}, u32[]{:S(2)}) copy-start(bf16[4096,256]{1,0:T(8,128)(2,1)} %param.23) | copy-start | bytes 6291460
  7.2 3.7 copy-start.2
  10.9 22.0 %copy-start.15 = (f32[1,512]{1,0:T(1,128)S(1)}, f32[1,512]{1,0:T(1,128)}, u32[]{:S(2)}) copy-start(f32[1,512]{1,0:T(1,128)} %param.20) | copy-start | bytes 6148
  10.9 23.1 %copy-start.12 = (f32[1,512]{1,0:T(1,128)S(1)}, f32[1,512]{1,0:T(1,128)}, u32[]{:S(2)}) copy-start(f32[1,512]{1,0:T(1,128)} %param.19) | copy-start | bytes 6148
  14.8 20.2 %copy-start.6 = (bf16[512,128]{1,0:T(8,128)(2,1)S(1)}, bf16[512,128]{1,0:T(8,128)(2,1)}, u32[]{:S(2)}) copy-start(bf16[512,128]{1,0:T(8,128)(2,1)} %param.17) | copy-start | bytes 393220
  14.8 21.0 %copy-start.5 = (bf16[512,256]{1,0:T(8,128)(2,1)S(1)}, bf16[512,256]{1,0:T(8,128)(2,1)}, u32[]{:S(2)}) copy-start(bf16[512,256]{1,0:T(8,128)(2,1)} %param.18) | copy-start | bytes 786436
  16.0 96.3 %all-to-all-start = ((bf16[32,32,256]{2,1,0:T(8,128)(2,1)}), bf16[32,32,256]{2,1,0:T(8,128)(2,1)}, u32[]{:S(2)}, u32[]{:S(2)}) async-start(bf16[32,32,256]{2,1,0:T(8,128)(2,1)} %select_select_fusion), calls=%async_computation | async-start | bytes 1048576 | tf_op jit(solution)/shard_map/all_to_all | solution.py:229
  32.8 145.0 %all-gather.9.cloned.1.call-start = ((), (), s32[]{:S(2)}) async-start(), calls=%async_computation.5 | async-start | bytes 2367488 | tf_op jit(solution)/shard_map/all_gather | solution.py:34
  33.4 2.4 copy-start.9
  35.0 2.2 copy-start.10
  117.4 94.1 %copy-start.17 = (f32[8,1]{0,1:T(1,128)S(1)}, f32[8,1]{0,1:T(1,128)}, u32[]{:S(2)}) copy-start(f32[8,1]{0,1:T(1,128)} %get-tuple-element.76) | copy-start | bytes 100
  117.4 94.1 %copy-start.18 = (f32[8,1]{0,1:T(1,128)S(1)}, f32[8,1]{0,1:T(1,128)}, u32[]{:S(2)}) copy-start(f32[8,1]{0,1:T(1,128)} %get-tuple-element.81) | copy-start | bytes 100
  117.4 94.2 %copy-start.13 = (f32[8,1,128]{2,1,0:T(1,128)S(1)}, f32[8,1,128]{2,1,0:T(1,128)}, u32[]{:S(2)}) copy-start(f32[8,1,128]{2,1,0:T(1,128)} %get-tuple-element.83) | copy-start | bytes 12292
  117.4 94.4 %copy-start.21 = (bf16[512,128]{1,0:T(8,128)(2,1)S(1)}, bf16[512,128]{1,0:T(8,128)(2,1)}, u32[]{:S(2)}) copy-start(bf16[512,128]{1,0:T(8,128)(2,1)} %param.16) | copy-start | bytes 393220
  117.4 94.7 %copy-start.7 = (bf16[512,128]{1,0:T(8,128)(2,1)S(1)}, bf16[512,128]{1,0:T(8,128)(2,1)}, u32[]{:S(2)}) copy-start(bf16[512,128]{1,0:T(8,128)(2,1)} %param.17) | copy-start | bytes 393220
  117.4 134.3 %all-to-all-start.1 = ((bf16[1024,16,256]{2,0,1:T(8,128)(2,1)}), bf16[1024,16,256]{2,0,1:T(8,128)(2,1)}, u32[]{:S(2)}, u32[]{:S(2)}) async-start(bf16[1024,16,256]{2,0,1:T(8,128)(2,1)} %concatenate.15), calls=%async_computation.1 | async-start | bytes 16777216 | tf_op jit(solution)/shard_map/all_to_all | solution.py:17
  124.4 202.7 %all-gather.7.cloned.1.call-start = ((), (), s32[]{:S(2)}) async-start(), calls=%async_computation.4 | async-start | bytes 4456448 | tf_op jit(solution)/shard_map/all_gather | solution.py:240
  211.8 3.0 copy-start.19
  251.7 17.6 %copy-start.3 = (bf16[1,64,4096]{2,1,0:T(8,128)(2,1)S(1)}, bf16[1,64,4096]{2,1,0:T(8,128)(2,1)}, u32[]{:S(2)}) copy-start(bf16[1,64,4096]{2,1,0:T(8,128)(2,1)} %param.27) | copy-start | bytes 1572868
  264.1 5.8 %copy-start.1 = (bf16[1024,16,256]{0,2,1:T(8,128)(2,1)S(1)}, bf16[1024,16,256]{0,2,1:T(8,128)(2,1)}, u32[]{:S(2)}) copy-start(bf16[1024,16,256]{0,2,1:T(8,128)(2,1)} %copy.70) | copy-start | bytes 25165828
  273.3 37.6 %copy-start.20 = (bf16[1,1024,256]{2,1,0:T(8,128)(2,1)S(1)}, bf16[1,1024,256]{2,1,0:T(8,128)(2,1)}, u32[]{:S(2)}) copy-start(bf16[1,1024,256]{2,1,0:T(8,128)(2,1)} %param.29) | copy-start | bytes 1572868
  310.9 15.3 %copy-start.11 = (s32[256,2]{0,1:T(2,128)S(1)}, s32[256,2]{0,1:T(2,128)}, u32[]{:S(2)}) copy-start(s32[256,2]{0,1:T(2,128)} %param.25) | copy-start | bytes 6148
  310.9 15.9 %copy-start.14 = (f32[256,2]{0,1:T(2,128)S(1)}, f32[256,2]{0,1:T(2,128)}, u32[]{:S(2)}) copy-start(f32[256,2]{0,1:T(2,128)} %param.26) | copy-start | bytes 6148
  312.5 47.1 %all-to-all-start.3 = ((bf16[32,32,256]{2,1,0:T(8,128)(2,1)}), bf16[32,32,256]{2,1,0:T(8,128)(2,1)S(1)}, u32[]{:S(2)}, u32[]{:S(2)}) async-start(bf16[32,32,256]{2,1,0:T(8,128)(2,1)} %bitcast.140), calls=%async_computation.3 | async-start | bytes 1048576 | tf_op jit(solution)/shard_map/all_to_all | solution.py:253
  (3 other events, 4.0 us)
Sparse Core Ops, SparseCore 0:
  112.4 65.3 all-gather.8
  216.7 100.4 all-gather.6
